TPU v7x, 32 devices: a whole 2x2x4 slice. The times are simulated.
32 devices in a mesh: ep: 8 (over z, x), tp: 4 (over y, core).
Axes of the slice: x: 2, y: 2, z: 4, core: 2. Of those that a mesh axis runs over, the one named last changes fastest.
Arguments:
- x_in: bfloat16 [4096, 3072], P('tp', 'ep'), may hold values from -6 to 6
- z_in: bfloat16 [4096, 3072], P('tp', 'ep'), may hold values from -6 to 6
- dt_raw: float32 [64, 3072], P('tp', 'ep'), may hold values from -6 to 6
- decay_rate: float32 [64], P('tp'), may hold values from 0 to 1, as said below
- b_in: bfloat16 [256, 3072], P(None, 'ep'), may hold values from -6 to 6
- c_in: bfloat16 [256, 3072], P(None, 'ep'), may hold values from -6 to 6
- conv_x: float32 [4096, 4], P('tp'), may hold values from -3 to 3
- conv_b: float32 [256, 4], replicated, may hold values from -3 to 3
- conv_c: float32 [256, 4], replicated, may hold values from -3 to 3
- head_gain: float32 [4096], P('tp'), may hold values from 0.1 to 1.9
- moe_rows: bfloat16 [1280, 2048], P('ep'), may hold values from -6 to 6
- moe_gain: float32 [2048], replicated, may hold values from 0.1 to 1.9
- routes: int32 [1280, 2], P('ep'), may hold values from 0 to 7, all different within a row; in each aligned block of 160 rows (0 to 159, 160 to 319, ...) at most 80 rows name the same one
- route_logit: float32 [1280, 2], P('ep'), may hold values from -6 to 6
- w_gate: bfloat16 [8, 2048, 5120], P('ep', None, 'tp'), may hold values from -0.125 to 0.125
- w_up: bfloat16 [8, 2048, 5120], P('ep', None, 'tp'), may hold values from -0.125 to 0.125
- w_down: bfloat16 [8, 5120, 2048], P('ep', 'tp'), may hold values from -0.078125 to 0.078125
Outputs:
- mixed: bfloat16 [4096, 3072], P('tp', 'ep')
- moe_out: bfloat16 [2048, 1280], P('tp', 'ep')
Inputs may be any that keep to these rules, and one draw needn't show every extreme that they name: `routes`: each row names 2 different experts; among the rows of one index of ep no expert is named more than 80 times, a bound that some block reaches. `decay_rate`: positive rates.
All inputs are finite; a program needn't handle non-finite values.
Results may differ from a plain program's by a relative error of at most 0.018.
Values may be sent and summed in bfloat16 or wider, within the bound.
No kernel may reach another device: no remote copies, remote signals or barrier semaphores. Data moves between devices by JAX's collectives and lax.ppermute only.
A program may use at most 64 MiB of HBM per device.

v0:
```python
import jax
import jax.numpy as jnp
from jax import lax
from jax.sharding import PartitionSpec as P

HEADS = 64
HEAD_DIM = 64
GROUPS = 2
NSTATE = 128
BLOCK = 128
EXP_DEV = 1
HIGHEST = lax.Precision.HIGHEST
ROW_EPS = 0.1
HEAD_EPS = 1.0


def from_behind(value, axis, steps):
    count = lax.axis_size(axis)
    initial, last = (max(0, -steps), min(count, count - steps))
    return lax.ppermute(value, axis, [(source, source + steps) for source in range(initial, last)])


def carried_in(shard, axis, join, neutral):
    place = lax.axis_index(axis)
    gathered = jax.tree.map(
        lambda a, kind: lax.all_gather(a.astype(kind), axis), shard, (jnp.bfloat16, jnp.bfloat16)
    )
    state = jax.tree.map(lambda a, e: jnp.zeros_like(a) + jnp.asarray(e, a.dtype), shard, neutral)

    def one(turn, state):
        return join(
            state,
            jax.tree.map(
                lambda a, own: lax.dynamic_index_in_dim(a, turn, 0, False).astype(own.dtype),
                gathered,
                shard,
            ),
        )

    return lax.fori_loop(0, place, one, state)


def conv_with_rims(signal, rim_rows, weight):
    taps = weight.shape[1]
    length = signal.shape[1]
    joined = jnp.concatenate([rim_rows.astype(jnp.float32), signal.astype(jnp.float32)], axis=1)
    running = jnp.zeros(signal.shape, jnp.float32)
    for offset in range(taps):
        running = running + weight[:, offset : offset + 1] * joined[:, offset : offset + length]
    return jax.nn.silu(running)


def block_step(state_in, x_block, b_block, c_block, log_block, step_block):
    cum_log = jnp.cumsum(log_block, axis=1)
    seg_log = cum_log[:, :, None] - cum_log[:, None, :]
    causal = jnp.tril(jnp.ones((log_block.shape[1], log_block.shape[1]), bool))
    decay_mask = jnp.exp(jnp.where(causal[None], seg_log, -jnp.inf))
    scores = (
        jnp.einsum("hnt,hns->hts", c_block, b_block, precision=HIGHEST)
        * decay_mask
        * step_block[:, None, :]
    )
    inner_term = jnp.einsum("hts,hps->hpt", scores, x_block, precision=HIGHEST)
    carried = (
        jnp.einsum("hnt,hpn->hpt", c_block, state_in, precision=HIGHEST)
        * jnp.exp(cum_log)[:, None, :]
    )
    tail_weight = jnp.exp(cum_log[:, -1:] - cum_log) * step_block
    fresh_state = jnp.einsum(
        "hps,hns->hpn", x_block * tail_weight[:, None, :], b_block, precision=HIGHEST
    )
    new_state = jnp.exp(cum_log[:, -1])[:, None, None] * state_in + fresh_state
    return (new_state, inner_term + carried)


def combine_states(before_part, after_part):
    return (
        before_part[0] * after_part[0],
        after_part[0][..., None, None] * before_part[1] + after_part[1],
    )


def mixer_half(x_in, z_in, dt_raw, decay_rate, b_in, c_in, conv_x, conv_b, conv_c, head_gain):
    head_count = dt_raw.shape[0]
    length = dt_raw.shape[1]
    taps = conv_x.shape[1]
    value_rows = x_in.shape[0]
    per_group = HEADS // GROUPS
    group_index = lax.axis_index("tp") * head_count // per_group
    b_own = lax.dynamic_slice_in_dim(b_in, group_index * NSTATE, NSTATE, 0)
    c_own = lax.dynamic_slice_in_dim(c_in, group_index * NSTATE, NSTATE, 0)
    taps_b = lax.dynamic_slice_in_dim(conv_b, group_index * NSTATE, NSTATE, 0)
    taps_c = lax.dynamic_slice_in_dim(conv_c, group_index * NSTATE, NSTATE, 0)
    edge = length - taps + 1
    own_rims = jnp.concatenate([x_in[:, edge:], b_own[:, edge:], c_own[:, edge:]], axis=0)
    rims = from_behind(own_rims, "ep", 1)
    x_conv = conv_with_rims(x_in, rims[:value_rows], conv_x).reshape(head_count, HEAD_DIM, length)
    b_conv = conv_with_rims(b_own, rims[value_rows : value_rows + NSTATE], taps_b)
    c_conv = conv_with_rims(c_own, rims[value_rows + NSTATE :], taps_c)
    step_dt = jax.nn.softplus(dt_raw)
    log_decay = -step_dt * decay_rate[:, None]
    block_count = length // BLOCK

    def blocks(tensor):
        return jnp.moveaxis(tensor.reshape(tensor.shape[:-1] + (block_count, BLOCK)), -2, 0)

    def spread_heads(tensor):
        return jnp.broadcast_to(tensor[None], (head_count,) + tensor.shape)

    def advance(state_in, inputs):
        x_block, b_block, c_block, log_block, step_block = inputs
        return block_step(
            state_in, x_block, spread_heads(b_block), spread_heads(c_block), log_block, step_block
        )

    init_state = jnp.zeros((head_count, HEAD_DIM, NSTATE), jnp.float32)
    local_state, block_out = lax.scan(
        advance,
        init_state,
        (blocks(x_conv), blocks(b_conv), blocks(c_conv), blocks(log_decay), blocks(step_dt)),
    )
    y_local = jnp.moveaxis(block_out, 0, -2).reshape(head_count, HEAD_DIM, length)
    total_decay = jnp.exp(jnp.sum(log_decay, axis=1))
    _, incoming = carried_in(
        (total_decay, local_state),
        "ep",
        combine_states,
        (jnp.ones_like(total_decay), jnp.zeros_like(local_state)),
    )
    reach_decay = jnp.exp(jnp.cumsum(log_decay, axis=1))
    carried = (
        jnp.einsum("nt,hpn->hpt", c_conv, incoming, precision=HIGHEST) * reach_decay[:, None, :]
    )
    y_mixed = y_local + carried
    gated_out = y_mixed * jax.nn.silu(
        z_in.astype(jnp.float32).reshape(head_count, HEAD_DIM, length)
    )
    head_scale = lax.rsqrt(jnp.mean(gated_out * gated_out, axis=1, keepdims=True) + HEAD_EPS)
    normed_out = gated_out * head_scale * head_gain.reshape(head_count, HEAD_DIM, 1)
    return normed_out.reshape(head_count * HEAD_DIM, length).astype(jnp.bfloat16)


def experts_half(moe_rows, moe_gain, routes, route_logit, w_gate, w_up, w_down):
    tokens = moe_rows.shape[0]
    top_count = routes.shape[1]
    features = moe_gain.shape[0]
    experts = EXP_DEV * lax.axis_size("ep")
    capacity = 2 * tokens * top_count // experts
    col_width = features // lax.axis_size("tp")
    rows_float = moe_rows.astype(jnp.float32)
    row_scale = lax.rsqrt(jnp.mean(rows_float * rows_float, axis=1, keepdims=True) + ROW_EPS)
    normed_float = rows_float * row_scale * moe_gain
    flat_routes = routes.reshape(-1)
    hit_table = (flat_routes[:, None] == jnp.arange(experts, dtype=jnp.int32)[None, :]).astype(
        jnp.int32
    )
    slot_rank = jnp.sum((jnp.cumsum(hit_table, axis=0) - hit_table) * hit_table, axis=1)
    slot_index = flat_routes * capacity + slot_rank
    owner_row = jnp.arange(tokens * top_count, dtype=jnp.int32) // top_count
    column = lax.axis_index("tp") * col_width
    normed = lax.dynamic_slice_in_dim(normed_float.astype(jnp.bfloat16), column, col_width, 1)
    outbox = (
        jnp.zeros((experts * capacity, col_width), jnp.bfloat16)
        .at[slot_index]
        .set(normed[owner_row])
    )
    arrived = lax.all_to_all(
        outbox.reshape(experts, capacity, col_width), "ep", split_axis=0, concat_axis=0, tiled=True
    ).reshape(-1, col_width)
    part_rows = lax.all_gather(arrived, "tp", axis=1, tiled=True)
    gate_rows = w_gate[0]
    up_rows = w_up[0]
    gate_act = jnp.dot(part_rows, gate_rows, preferred_element_type=jnp.float32)
    up_act = jnp.dot(part_rows, up_rows, preferred_element_type=jnp.float32)
    hidden = (jax.nn.silu(gate_act) * up_act).astype(jnp.bfloat16)
    columns = w_down[0]
    summed = lax.psum_scatter(
        lax.dot_general(
            columns, hidden, (((0,), (1,)), ((), ())), preferred_element_type=jnp.float32
        ).astype(jnp.bfloat16),
        "tp",
        scatter_dimension=0,
        tiled=True,
    )
    expert_out = summed.reshape(col_width, experts, capacity)
    returned = lax.all_to_all(expert_out, "ep", split_axis=1, concat_axis=1, tiled=True)
    picked = returned.reshape(col_width, experts * capacity)[:, slot_index].astype(jnp.float32)
    picked = picked.reshape(col_width, tokens, top_count)
    weight = jax.nn.sigmoid(route_logit - route_logit[:, ::-1])
    combined = jnp.sum(picked * weight[None], axis=2)
    return combined.astype(jnp.bfloat16)


def on_device(
    x_in,
    z_in,
    dt_raw,
    decay_rate,
    b_in,
    c_in,
    conv_x,
    conv_b,
    conv_c,
    head_gain,
    moe_rows,
    moe_gain,
    routes,
    route_logit,
    w_gate,
    w_up,
    w_down,
):
    mixed = mixer_half(
        x_in, z_in, dt_raw, decay_rate, b_in, c_in, conv_x, conv_b, conv_c, head_gain
    )
    moe_out = experts_half(moe_rows, moe_gain, routes, route_logit, w_gate, w_up, w_down)
    return (mixed, moe_out)


def solution(mesh):
    return jax.shard_map(
        on_device,
        mesh=mesh,
        in_specs=(
            P("tp", "ep"),
            P("tp", "ep"),
            P("tp", "ep"),
            P("tp"),
            P(None, "ep"),
            P(None, "ep"),
            P("tp", None),
            P(),
            P(),
            P("tp"),
            P("ep", None),
            P(),
            P("ep", None),
            P("ep", None),
            P("ep", None, "tp"),
            P("ep", None, "tp"),
            P("ep", "tp", None),
        ),
        out_specs=(P("tp", "ep"), P("tp", "ep")),
        check_vma=False,
    )
```

profile of v0, /device:TPU:31, one launch (start us, length us, event | category | flops | bytes accessed | tf_op | source)
XLA Modules:
  0.0 211.8 jit_solution(18337351531180557523)
XLA Ops:
  8.1 1.3 convert_element_type.100
  9.9 0.9 reduce-window.16
  11.4 0.8 dynamic-slice.1
  12.3 3.4 %scatter_custom_fusion = bf16[640,512]{1,0:T(8,128)(2,1)S(1)} fusion(s32[320]{0:T(512)S(1)} %get-tuple-element.186, bf16[160,512]{1,0:T(8,128)(2,1)S(1)} %fusion.45, s32[1024]{0:T(1024)S(1)} %pad_clamp_fusion.1, bf16[]{:T(256)} %constant.124.clone.1), kind=kCustom, calls=%fused_computation.70 | custom fusion | bytes 655362 | tf_op jit(solution)/shard_map/scatter | solution.py:165
  15.8 20.8 %all_to_all.10 = bf16[8,80,512]{2,1,0:T(8,128)(2,1)} all-to-all(bf16[8,80,512]{2,1,0:T(8,128)(2,1)S(1)} %bitcast.153), channel_id=1, replica_groups=mesh['ep'=8,'tp'=4] {'ep'}, dimensions={0} | all-to-all | bytes 1310720 | tf_op jit(solution)/shard_map/all_to_all | solution.py:167
  37.3 1.5 collective-permute-start
  38.9 0.7 fusion.73
  39.6 0.6 slice_bitcast_fusion.3
  40.4 0.6 reshape.229
  41.0 0.7 collective-permute-done
  42.0 3.2 %divide_multiply_fusion = f32[1024,384]{1,0:T(8,128)} fusion(f32[1024,384]{1,0:T(8,128)S(1)} %convert_element_type.89, f32[1024,3]{1,0:T(8,128)S(1)} %copy.41, f32[1024]{0:T(1024)S(1)} %bitcast.164, f32[1024]{0:T(1024)S(1)} %bitcast.165, f32[1024]{0:T(1024)S(1)} %bitcast.163, f32[1024]{0:T(1024)S(1)} %bitcast.162), kind=kLoop, calls=%fused_computation.63 | loop fusion | flops 5505024 | bytes 3174400 | tf_op jit(solution)/shard_map/jit(silu)/mul | solution.py:50
  45.2 2.6 %reshape_reshape.3 = f32[16,64,3,128]{3,2,1,0:T(4,128)S(1)} reshape(f32[1024,384]{1,0:T(8,128)} %divide_multiply_fusion) | data formatting | bytes 3145728 | tf_op jit(solution)/shard_map/reshape;reshape | solution.py:105
  48.1 14.7 %all-gather.5.cloned.1.call-done = bf16[640,2048]{1,0:T(8,128)(2,1)} async-done(((bf16[640,512]{1,0:T(8,128)(2,1)}), bf16[640,2048]{1,0:T(8,128)(2,1)}) %all-gather.5.cloned.1.call-update) | async-done | bytes 2621456 | tf_op jit(solution)/shard_map/all_gather | solution.py:170
  62.8 8.5 %fusion.18 = f32[640,1280]{1,0:T(8,128)} fusion(bf16[640,2048]{1,0:T(8,128)(2,1)} %all-gather.5.cloned.1.call-done, bf16[1,2048,1280]{2,1,0:T(8,128)(2,1)} %param.35), kind=kOutput, calls=%fused_computation.35 | convolution fusion | flops 3355443200 | bytes 11141120 | tf_op jit(solution)/shard_map/dot_general | solution.py:173
  71.3 15.2 %fusion.29 = bf16[2048,640]{0,1:T(8,128)(2,1)} fusion(bf16[1,1280,2048]{2,1,0:T(8,128)(2,1)} %param.37, bf16[640,2048]{1,0:T(8,128)(2,1)} %all-gather.5.cloned.1.call-done, bf16[1,2048,1280]{2,1,0:T(8,128)(2,1)} %param.36, f32[640,1280]{1,0:T(8,128)} %fusion.18), kind=kOutput, calls=%fused_computation.40 | convolution fusion | flops 6717112320 | bytes 19005440 | tf_op jit(solution)/shard_map/dot_general | solution.py:178
  86.8 40.6 %while.26 = (s32[]{:T(128)}, f32[16,64,128]{2,1,0:T(8,128)S(1)}, f32[3,16,64,128]{3,2,1,0:T(8,128)}, f32[3,16,128]{2,0,1:T(4,128)S(1)}, f32[3,16,64,128]{3,0,2,1...) while((s32[]{:T(128)}, f32[16,64,128]{2,1,0:T(8,128)S(1)}, ...), condition=%wide.region_2.3_spmd.clone, body=%wide.region_0.2_spmd.clone.sunk | while | flops 1008879616 | bytes 10045104 | solution.py:117
  86.8 1.4 constant_dynamic-slice_fusion.14
  88.2 0.3 reduce_window_sum.51
  88.7 1.3 fusion.103
  90.1 1.6 fusion.104
  91.9 2.7 %fusion.105 = f32[16,128,128]{2,1,0:T(8,128)S(1)} fusion(f32[16,128]{1,0:T(8,128)} %bitcast.142, f32[16,128]{1,0:T(8,128)S(1)} %reduce_window_sum.51, f32[128,128]{1,0:T(8,128)S(1)} %bitcast.151, f32[128,128]{1,0:T(8,128)S(1)} %bitcast.148, pred[128,128]{1,0:T(8,128)(4,1)S(1)} %iota_compare_fusion.4), kind=kOutput, calls=%fused_computation.6.clone.1 | convolution fusion | flops 403701760 | bytes 1212416 | tf_op jit(solution)/shard_map/while/body/eval_jaxpr/hnt,hns->hts/dot_general | solution.py:59
  94.6 0.6 constant_dynamic-slice_fusion.13
  95.2 3.0 %fusion.106 = f32[3,16,64,128]{3,2,1,0:T(8,128)} fusion(f32[3,16,64,128]{3,2,1,0:T(8,128)} %get-tuple-element.298, s32[]{:T(128)} %get-tuple-element.296, f32[16,64,128]{2,1,0:T(8,128)S(1)} %fusion.104, f32[16,64,128]{2,1,0:T(8,128)S(1)} %bitcast.144, f32[16,128,128]{2,1,0:T(8,128)S(1)} %fusion.105), kind=kOutput, calls=%fused_computation.11.clone.1 | convolution fusion | flops 201457664 | bytes 2621952 | tf_op jit(solution)/shard_map/while/body/eval_jaxpr/hts,hps->hpt/dot_general | solution.py:63
  98.2 2.1 %convolution_add_fusion.3 = f32[16,64,128]{2,1,0:T(8,128)S(1)} fusion(f32[128,128]{1,0:T(8,128)S(1)} %bitcast.149, f32[16,64,128]{2,1,0:T(8,128)S(1)} %bitcast.145, f32[16,64,128]{2,1,0:T(8,128)S(1)} %get-tuple-element.297, f32[16,128]{1,0:T(8,128)S(1)} %get-tuple-element.282, f32[16]{0:T(128)S(1)} %exp.118, pred[]{:T(512)S(6)} %compare.10), kind=kOutput, calls=%fused_computation.12.clone.1 | convolution fusion | flops 201850880 | bytes 1646657 | tf_op jit(solution)/shard_map/while/body/eval_jaxpr/hps,hns->hpn/dot_general | solution.py:69
  100.4 1.4 constant_dynamic-slice_fusion.14
  101.8 0.3 reduce_window_sum.51
  102.3 1.3 fusion.103
  103.7 1.6 fusion.104
  105.5 2.7 %fusion.105 = f32[16,128,128]{2,1,0:T(8,128)S(1)} fusion(f32[16,128]{1,0:T(8,128)} %bitcast.142, f32[16,128]{1,0:T(8,128)S(1)} %reduce_window_sum.51, f32[128,128]{1,0:T(8,128)S(1)} %bitcast.151, f32[128,128]{1,0:T(8,128)S(1)} %bitcast.148, pred[128,128]{1,0:T(8,128)(4,1)S(1)} %iota_compare_fusion.4), kind=kOutput, calls=%fused_computation.6.clone.1 | convolution fusion | flops 403701760 | bytes 1212416 | tf_op jit(solution)/shard_map/while/body/eval_jaxpr/hnt,hns->hts/dot_general | solution.py:59
  108.2 0.6 constant_dynamic-slice_fusion.13
  108.8 3.0 %fusion.106 = f32[3,16,64,128]{3,2,1,0:T(8,128)} fusion(f32[3,16,64,128]{3,2,1,0:T(8,128)} %get-tuple-element.298, s32[]{:T(128)} %get-tuple-element.296, f32[16,64,128]{2,1,0:T(8,128)S(1)} %fusion.104, f32[16,64,128]{2,1,0:T(8,128)S(1)} %bitcast.144, f32[16,128,128]{2,1,0:T(8,128)S(1)} %fusion.105), kind=kOutput, calls=%fused_computation.11.clone.1 | convolution fusion | flops 201457664 | bytes 2621952 | tf_op jit(solution)/shard_map/while/body/eval_jaxpr/hts,hps->hpt/dot_general | solution.py:63
  111.8 2.1 convolution_add_fusion.3
  113.9 1.4 constant_dynamic-slice_fusion.14
  115.8 1.3 fusion.103
  117.2 1.6 fusion.104
  119.0 2.7 %fusion.105 = f32[16,128,128]{2,1,0:T(8,128)S(1)} fusion(f32[16,128]{1,0:T(8,128)} %bitcast.142, f32[16,128]{1,0:T(8,128)S(1)} %reduce_window_sum.51, f32[128,128]{1,0:T(8,128)S(1)} %bitcast.151, f32[128,128]{1,0:T(8,128)S(1)} %bitcast.148, pred[128,128]{1,0:T(8,128)(4,1)S(1)} %iota_compare_fusion.4), kind=kOutput, calls=%fused_computation.6.clone.1 | convolution fusion | flops 403701760 | bytes 1212416 | tf_op jit(solution)/shard_map/while/body/eval_jaxpr/hnt,hns->hts/dot_general | solution.py:59
  121.7 0.6 constant_dynamic-slice_fusion.13
  122.3 2.9 %fusion.106 = f32[3,16,64,128]{3,2,1,0:T(8,128)} fusion(f32[3,16,64,128]{3,2,1,0:T(8,128)} %get-tuple-element.298, s32[]{:T(128)} %get-tuple-element.296, f32[16,64,128]{2,1,0:T(8,128)S(1)} %fusion.104, f32[16,64,128]{2,1,0:T(8,128)S(1)} %bitcast.144, f32[16,128,128]{2,1,0:T(8,128)S(1)} %fusion.105), kind=kOutput, calls=%fused_computation.11.clone.1 | convolution fusion | flops 201457664 | bytes 2621952 | tf_op jit(solution)/shard_map/while/body/eval_jaxpr/hts,hps->hpt/dot_general | solution.py:63
  125.3 2.1 convolution_add_fusion.3
  127.4 0.7 convert_element_type.96
  128.2 1.3 dynamic-slice
  130.2 0.6 exponential_convert_fusion
  131.0 13.7 %all-reduce.1 = bf16[128]{0:T(256)(128)(2,1)S(1)} all-reduce(bf16[128]{0:T(256)(128)(2,1)S(1)} %dynamic-update-slice), channel_id=2, replica_groups=mesh['ep'=8,'tp'=4] {'ep'}, use_global_device_ids=true, to_apply=%add.1 | all-reduce | flops 128 | bytes 512
  144.8 0.7 copy_bitcast_fusion.1
  145.6 0.9 reduce-window.14
  146.6 0.8 mul.348
  147.4 0.7 rev.3
  148.1 0.7 add_divide_fusion
  148.9 0.6 pad_clamp_fusion
  149.7 7.9 %all-to-all-start.1 = ((bf16[512,8,80]{0,2,1:T(8,128)(2,1)}), bf16[512,8,80]{0,2,1:T(8,128)(2,1)S(1)}, u32[]{:S(2)}, u32[]{:S(2)}) async-start(bf16[512,8,80]{0,2,1:T(8,128)(2,1)} %bitcast.160), calls=%async_computation.2 | async-start | bytes 1310720 | tf_op jit(solution)/shard_map/all_to_all | solution.py:186
  157.6 30.3 %all-gather.7.cloned.1.call-done = bf16[128,64,128]{2,1,0:T(8,128)(2,1)} async-done(((bf16[16,64,128]{2,1,0:T(8,128)(2,1)}), bf16[128,64,128]{2,1,0:T(8,128)(2,1)}) %all-gather.7.cloned.1.call-update) | async-done | bytes 2097168 | tf_op jit(solution)/shard_map/all_gather | solution.py:26
  187.9 8.2 %while.25 = (s32[]{:T(128)}, f32[16,64,128]{2,1,0:T(8,128)S(1)}, s32[]{:T(128)}, bf16[8,16]{1,0:T(8,128)(2,1)S(1)}, bf16[8,16,64,128]{3,2,1,0:T(8,128)(2,1)}, /*index=5*/s32[]{:T(128)}, s32[]{:T(128)}, s32[]{:T(128)}) while((s32[]{:T(128)}, f32[16,64,128]{2,1,0:T(8,128)S(1)}, s32[]{:T(128)}, bf16[8,16]{1,0:T(8,128)(2,1)S(1)}, ...), condition=%wide.region_5.6_spmd, body=%wide.region_4.5_spmd.sunk | while | flops 393237 | bytes 1311007 | solution.py:40
  188.0 1.2 convert_add_fusion.2
  189.2 1.1 convert_add_fusion.2
  190.4 1.1 convert_add_fusion.2
  191.6 1.1 convert_add_fusion.2
  192.7 1.1 convert_add_fusion.2
  193.9 1.1 convert_add_fusion.2
  195.0 1.1 convert_add_fusion.2
  196.2 3.0 %multiply_reduce_fusion = (f32[16,384]{1,0:T(8,128)S(1)}, f32[16,64,384]{2,1,0:T(8,128)S(1)}) fusion(bf16[16,64,384]{2,1,0:T(8,128)(2,1)} %bitcast.168, f32[16,384]{1,0:T(8,128)S(1)} %copy_bitcast_fusion, f32[16,64,128]{2,1,0:T(8,128)S(1)} %get-tuple-element.91, f32[128,384]{0,1:T(8,128)S(1)} %bitcast.155, f32[3,16,64,128]{3,2,1,0:T(8,128)S(1)} %copy-done.20), kind=kOutput, calls=%fused_computation.62 | convolution fusion | flops 607905792 | bytes 4702208 | tf_op jit(solution)/shard_map/nt,hpn->hpt/dot_general | solution.py:132
  199.2 1.1 multiply_convert_fusion
  200.4 2.0 gather_fusion
  202.5 0.4 reshape.247
  202.8 1.5 multiply_reduce_fusion.2
  (148 shorter events, 5.4 us)
Async XLA Ops:
  8.0 1.3 copy-start
  8.0 1.6 copy-start.14
  8.0 54.8 %all-gather.5.cloned.1.call-start = ((), (), s32[]{:S(2)}) async-start(), calls=%async_computation.3 | async-start | bytes 3276800 | tf_op jit(solution)/shard_map/all_gather | solution.py:170
  11.4 25.2 %copy-start.13 = (s32[320]{0:T(512)}, s32[320]{0:T(512)S(1)}, u32[]{:S(2)}) copy-start(s32[320]{0:T(512)S(1)} %get-tuple-element.186) | copy-start | bytes 3844
  12.2 24.5 %copy-start.9 = (bf16[256,384]{1,0:T(8,128)(2,1)S(1)}, bf16[256,384]{1,0:T(8,128)(2,1)}, u32[]{:S(2)}) copy-start(bf16[256,384]{1,0:T(8,128)(2,1)} %param.26) | copy-start | bytes 589828
  12.2 24.5 %copy-start.10 = (bf16[256,384]{1,0:T(8,128)(2,1)S(1)}, bf16[256,384]{1,0:T(8,128)(2,1)}, u32[]{:S(2)}) copy-start(bf16[256,384]{1,0:T(8,128)(2,1)} %param.25) | copy-start | bytes 589828
  12.3 24.7 %copy-start.1 = (bf16[1024,384]{1,0:T(8,128)(2,1)S(1)}, bf16[1024,384]{1,0:T(8,128)(2,1)}, u32[]{:S(2)}) copy-start(bf16[1024,384]{1,0:T(8,128)(2,1)} %param.21) | copy-start | bytes 2359300
  15.7 23.1 %copy-start.17 = (f32[256,4]{0,1:T(4,128)S(1)}, f32[256,4]{0,1:T(4,128)}, u32[]{:S(2)}) copy-start(f32[256,4]{0,1:T(4,128)} %param.29) | copy-start | bytes 12292
  15.7 23.1 %copy-start.18 = (f32[256,4]{0,1:T(4,128)S(1)}, f32[256,4]{0,1:T(4,128)}, u32[]{:S(2)}) copy-start(f32[256,4]{0,1:T(4,128)} %param.28) | copy-start | bytes 12292
  15.7 23.1 %copy-start.12 = (f32[1024,4]{0,1:T(4,128)S(1)}, f32[1024,4]{0,1:T(4,128)}, u32[]{:S(2)}) copy-start(f32[1024,4]{0,1:T(4,128)} %param.27) | copy-start | bytes 49156
  15.7 23.1 %copy-start.11 = (f32[16,384]{1,0:T(8,128)S(1)}, f32[16,384]{1,0:T(8,128)}, u32[]{:S(2)}) copy-start(f32[16,384]{1,0:T(8,128)} %param.23) | copy-start | bytes 73732
  15.7 23.1 %copy-start.19 = (f32[16]{0:T(128)S(1)}, f32[16]{0:T(128)}, u32[]{:S(2)}) copy-start(f32[16]{0:T(128)} %param.24) | copy-start | bytes 196
  36.6 113.1 %reduce-scatter.2.cloned.1.call-start = ((), (), s32[]{:S(2)}) async-start(), calls=%async_computation.4 | async-start | bytes 3276800 | tf_op jit(solution)/shard_map/reduce_scatter | solution.py:177
  37.3 4.4 %collective-permute-start = (bf16[1280,3]{0,1:T(4,128)(2,1)S(1)}, bf16[1280,3]{0,1:T(4,128)(2,1)S(1)}, u32[]{:S(2)}, u32[]{:S(2)}) collective-permute-start(bf16[1280,3]{0,1:T(4,128)(2,1)S(1)} %pad_maximum_fusion.3), channel_id=1, source_target_pairs={{0,4},{4,8},{8,12},{12,16},{16,20},{20,24},{24,28},{1,5},{5,9},{9,... | collective-permute-start | bytes 23048 | tf_op jit(solution)/shard_map/ppermute | solution.py:20
  39.6 2.3 %copy-start.4 = (f32[16,384]{1,0:T(8,128)}, f32[16,384]{1,0:T(8,128)S(1)}, u32[]{:S(2)}) copy-start(f32[16,384]{1,0:T(8,128)S(1)} %get-tuple-element.162) | copy-start | bytes 73732
  45.2 2.8 %copy-start.15 = (f32[128]{0:T(128)S(1)}, f32[128]{0:T(128)}, u32[]{:S(2)}) copy-start(f32[128]{0:T(128)} %get-tuple-element.178) | copy-start | bytes 1540
  45.2 2.8 %copy-start.16 = (f32[128]{0:T(128)S(1)}, f32[128]{0:T(128)}, u32[]{:S(2)}) copy-start(f32[128]{0:T(128)} %get-tuple-element.179) | copy-start | bytes 1540
  86.5 101.4 %all-gather.7.cloned.1.call-start = ((), (), s32[]{:S(2)}) async-start(), calls=%async_computation.5 | async-start | bytes 2359296 | tf_op jit(solution)/shard_map/all_gather | solution.py:26
  86.8 3.2 %copy-start.5 = (f32[3,16,128]{2,0,1:T(4,128)}, f32[3,16,128]{2,0,1:T(4,128)S(1)}, u32[]{:S(2)}) copy-start(f32[3,16,128]{2,0,1:T(4,128)S(1)} %get-tuple-element.310) | copy-start | bytes 73732 | tf_op jit(solution)/shard_map/while
  86.8 3.3 %copy-start.2 = (f32[3,128,128]{1,2,0:T(8,128)}, f32[3,128,128]{1,2,0:T(8,128)S(1)}, u32[]{:S(2)}) copy-start(f32[3,128,128]{1,2,0:T(8,128)S(1)} %get-tuple-element.313) | copy-start | bytes 589828 | tf_op jit(solution)/shard_map/while
  88.7 1.3 copy-start.7
  95.2 3.0 %copy-start.8 = (f32[16]{0:T(128)S(1)}, f32[16]{0:T(128)}, u32[]{:S(2)}) copy-start(f32[16]{0:T(128)} %copy-done.7) | copy-start | bytes 196 | tf_op jit(solution)/shard_map/while
  95.2 5.1 %copy-start.6 = (f32[3,16,128]{2,0,1:T(4,128)S(1)}, f32[3,16,128]{2,0,1:T(4,128)}, u32[]{:S(2)}) copy-start(f32[3,16,128]{2,0,1:T(4,128)} %copy-done.5) | copy-start | bytes 73732 | tf_op jit(solution)/shard_map/while
  98.2 2.2 %copy-start.3 = (f32[3,128,128]{1,2,0:T(8,128)S(1)}, f32[3,128,128]{1,2,0:T(8,128)}, u32[]{:S(2)}) copy-start(f32[3,128,128]{1,2,0:T(8,128)} %copy-done.2) | copy-start | bytes 589828 | tf_op jit(solution)/shard_map/while
  100.4 3.2 %copy-start.5 = (f32[3,16,128]{2,0,1:T(4,128)}, f32[3,16,128]{2,0,1:T(4,128)S(1)}, u32[]{:S(2)}) copy-start(f32[3,16,128]{2,0,1:T(4,128)S(1)} %get-tuple-element.310) | copy-start | bytes 73732 | tf_op jit(solution)/shard_map/while
  100.4 3.3 %copy-start.2 = (f32[3,128,128]{1,2,0:T(8,128)}, f32[3,128,128]{1,2,0:T(8,128)S(1)}, u32[]{:S(2)}) copy-start(f32[3,128,128]{1,2,0:T(8,128)S(1)} %get-tuple-element.313) | copy-start | bytes 589828 | tf_op jit(solution)/shard_map/while
  102.3 1.3 copy-start.7
  108.7 3.0 %copy-start.8 = (f32[16]{0:T(128)S(1)}, f32[16]{0:T(128)}, u32[]{:S(2)}) copy-start(f32[16]{0:T(128)} %copy-done.7) | copy-start | bytes 196 | tf_op jit(solution)/shard_map/while
  108.7 5.1 %copy-start.6 = (f32[3,16,128]{2,0,1:T(4,128)S(1)}, f32[3,16,128]{2,0,1:T(4,128)}, u32[]{:S(2)}) copy-start(f32[3,16,128]{2,0,1:T(4,128)} %copy-done.5) | copy-start | bytes 73732 | tf_op jit(solution)/shard_map/while
  111.7 2.2 %copy-start.3 = (f32[3,128,128]{1,2,0:T(8,128)S(1)}, f32[3,128,128]{1,2,0:T(8,128)}, u32[]{:S(2)}) copy-start(f32[3,128,128]{1,2,0:T(8,128)} %copy-done.2) | copy-start | bytes 589828 | tf_op jit(solution)/shard_map/while
  113.9 3.2 %copy-start.5 = (f32[3,16,128]{2,0,1:T(4,128)}, f32[3,16,128]{2,0,1:T(4,128)S(1)}, u32[]{:S(2)}) copy-start(f32[3,16,128]{2,0,1:T(4,128)S(1)} %get-tuple-element.310) | copy-start | bytes 73732 | tf_op jit(solution)/shard_map/while
  113.9 3.3 %copy-start.2 = (f32[3,128,128]{1,2,0:T(8,128)}, f32[3,128,128]{1,2,0:T(8,128)S(1)}, u32[]{:S(2)}) copy-start(f32[3,128,128]{1,2,0:T(8,128)S(1)} %get-tuple-element.313) | copy-start | bytes 589828 | tf_op jit(solution)/shard_map/while
  115.8 1.3 copy-start.7
  122.3 3.0 %copy-start.8 = (f32[16]{0:T(128)S(1)}, f32[16]{0:T(128)}, u32[]{:S(2)}) copy-start(f32[16]{0:T(128)} %copy-done.7) | copy-start | bytes 196 | tf_op jit(solution)/shard_map/while
  122.3 5.1 %copy-start.6 = (f32[3,16,128]{2,0,1:T(4,128)S(1)}, f32[3,16,128]{2,0,1:T(4,128)}, u32[]{:S(2)}) copy-start(f32[3,16,128]{2,0,1:T(4,128)} %copy-done.5) | copy-start | bytes 73732 | tf_op jit(solution)/shard_map/while
  125.3 2.2 %copy-start.3 = (f32[3,128,128]{1,2,0:T(8,128)S(1)}, f32[3,128,128]{1,2,0:T(8,128)}, u32[]{:S(2)}) copy-start(f32[3,128,128]{1,2,0:T(8,128)} %copy-done.2) | copy-start | bytes 589828 | tf_op jit(solution)/shard_map/while
  149.7 50.7 %all-to-all-start.1 = ((bf16[512,8,80]{0,2,1:T(8,128)(2,1)}), bf16[512,8,80]{0,2,1:T(8,128)(2,1)S(1)}, u32[]{:S(2)}, u32[]{:S(2)}) async-start(bf16[512,8,80]{0,2,1:T(8,128)(2,1)} %bitcast.160), calls=%async_computation.2 | async-start | bytes 1310720 | tf_op jit(solution)/shard_map/all_to_all | solution.py:186
  187.9 8.3 %copy-start.20 = (f32[3,16,64,128]{3,2,1,0:T(8,128)S(1)}, f32[3,16,64,128]{3,2,1,0:T(8,128)}, u32[]{:S(2)}) copy-start(f32[3,16,64,128]{3,2,1,0:T(8,128)} %get-tuple-element.89) | copy-start | bytes 4718596
Sparse Core Ops, SparseCore 0:
  36.7 26.0 all-gather.4
  86.6 33.8 reduce-scatter.1
Sparse Core Ops, SparseCore 1:
  128.3 59.6 all-gather.6
where the time goes:
time: 213 us; the launch traced here: 212 us
  matrix products  55.1 us (26%)
  waiting for transfers between devices  45.8 us (22%)
  blocking collectives  34.5 us (16%)
  other arithmetic  26.1 us (12%)
  local copies, waits for them, and re-layouts  23.2 us (11%)
  between operations  16.7 us (8%)
  starting transfers between devices  9.75 us (5%)
    all_gather x1, waiting for transfers between devices, carried_in(): lax.all_gather(a.astype(kind), axis)  30.3 us
    all_to_all x1, blocking collectives, experts_half(): lax.all_to_all(outbox.reshape(experts, capacity, col_width), 'ep', split_...  20.8 us
    dot_general x1, matrix products, experts_half(): lax.dot_general(columns, hidden, (((0,), (1,)), ((), ())), preferred_elem...  15.2 us
    all_gather x1, waiting for transfers between devices, experts_half(): part_rows = lax.all_gather(arrived, 'tp', axis=1, tiled=True)  14.7 us
    unnamed x1, blocking collectives  13.7 us
    dot_general x3, matrix products, block_step(): inner_term = jnp.einsum('hts,hps->hpt', scores, x_block, precision=HIGHEST)  8.92 us
    dot_general x1, matrix products, experts_half(): gate_act = jnp.dot(part_rows, gate_rows, preferred_element_type=jnp.float32)  8.51 us
    dot_general x3, matrix products, block_step(): jnp.einsum('hnt,hns->hts', c_block, b_block, precision=HIGHEST) * decay_mask  8.14 us
  transfers between devices with their start and end apart: 5, of which 3 were waited for; matrix products, arithmetic and copies ran while one was open for 33% of the time, Pallas kernels for 0%

commit v1 on v0

--- a/solution.py
+++ b/solution.py
@@ -167,7 +167,7 @@
     arrived = lax.all_to_all(
         outbox.reshape(experts, capacity, col_width), "ep", split_axis=0, concat_axis=0, tiled=True
     ).reshape(-1, col_width)
-    part_rows = lax.all_gather(arrived, "tp", axis=1, tiled=True)
+    part_rows = jnp.concatenate(lax.all_gather(arrived, "tp"), axis=1)
     gate_rows = w_gate[0]
     up_rows = w_up[0]
     gate_act = jnp.dot(part_rows, gate_rows, preferred_element_type=jnp.float32)

time: 213 us -> 209 us (0.981)
  matrix products: 55.1 us -> 49.8 us
  local copies, waits for them, and re-layouts: 23.2 us -> 26.6 us
    dot_general x1, matrix products: 15.2 us -> 4.82 us  [experts_half(): lax.dot_general(columns, hidden, (((0,), (1,)), ((), ())), preferred_elem...]
    dot_general x0 -> x1, matrix products: none -> 6.54 us  [experts_half(): up_act = jnp.dot(part_rows, up_rows, preferred_element_type=jnp.float32)]
    all_gather x0 -> x1, local copies, waits for them, and re-layouts: none -> 4.4 us  [experts_half(): part_rows = jnp.concatenate(lax.all_gather(arrived, 'tp'), axis=1)]
  transfers between devices with their start and end apart: 5 -> 5, of which waited for: 3 -> 3; matrix products, arithmetic and copies ran while one was open for 33% -> 32% of each run, Pallas kernels for 0% -> 0%
where the time goes in v1:
time: 209 us; the launch traced here: 207 us
  matrix products  49.8 us (24%)
  waiting for transfers between devices  45.1 us (22%)
  blocking collectives  34.4 us (16%)
  local copies, waits for them, and re-layouts  26.6 us (13%)
  other arithmetic  24.2 us (12%)
  between operations  16.8 us (8%)
  starting transfers between devices  9.75 us (5%)
    all_gather x1, waiting for transfers between devices, carried_in(): lax.all_gather(a.astype(kind), axis)  30.2 us
    all_to_all x1, blocking collectives, experts_half(): lax.all_to_all(outbox.reshape(experts, capacity, col_width), 'ep', split_...  20.8 us
    all_gather x1, waiting for transfers between devices, experts_half(): part_rows = jnp.concatenate(lax.all_gather(arrived, 'tp'), axis=1)  14.7 us
    unnamed x1, blocking collectives  13.6 us
    dot_general x3, matrix products, block_step(): inner_term = jnp.einsum('hts,hps->hpt', scores, x_block, precision=HIGHEST)  8.88 us
    dot_general x3, matrix products, block_step(): jnp.einsum('hnt,hns->hts', c_block, b_block, precision=HIGHEST) * decay_mask  8.14 us
    all_to_all x1, starting transfers between devices, experts_half(): lax.all_to_all(expert_out, 'ep', split_axis=1, concat_axis=1, tiled=True)  7.93 us
    add x7, other arithmetic, combine_states(): after_part[0][..., None, None] * before_part[1] + after_part[1]  7.88 us
  transfers between devices with their start and end apart: 5, of which 3 were waited for; matrix products, arithmetic and copies ran while one was open for 32% of the time, Pallas kernels for 0%

profile of v1, /device:TPU:31, one launch (start us, length us, event | category | flops | bytes accessed | tf_op | source)
XLA Modules:
  0.0 207.2 jit_solution(14683823329358027904)
XLA Ops:
  8.1 1.3 convert_element_type.100
  9.9 0.9 reduce-window.16
  11.4 0.8 dynamic-slice.1
  12.3 3.4 %scatter_custom_fusion = bf16[640,512]{1,0:T(8,128)(2,1)S(1)} fusion(s32[320]{0:T(512)S(1)} %get-tuple-element.194, bf16[160,512]{1,0:T(8,128)(2,1)S(1)} %fusion.45, s32[1024]{0:T(1024)S(1)} %pad_clamp_fusion.1, bf16[]{:T(256)} %constant.124.clone.1), kind=kCustom, calls=%fused_computation.70 | custom fusion | bytes 655362 | tf_op jit(solution)/shard_map/scatter | solution.py:165
  15.8 20.8 %all_to_all.10 = bf16[8,80,512]{2,1,0:T(8,128)(2,1)} all-to-all(bf16[8,80,512]{2,1,0:T(8,128)(2,1)S(1)} %bitcast.157), channel_id=1, replica_groups=mesh['ep'=8,'tp'=4] {'ep'}, dimensions={0} | all-to-all | bytes 1310720 | tf_op jit(solution)/shard_map/all_to_all | solution.py:167
  37.3 1.5 collective-permute-start
  38.9 0.8 fusion.70
  39.6 0.6 slice_bitcast_fusion.3
  40.4 0.6 reshape.231
  41.0 0.6 reshape.232
  42.0 3.2 %divide_multiply_fusion = f32[1024,384]{1,0:T(8,128)} fusion(f32[1024,384]{1,0:T(8,128)S(1)} %convert_element_type.89, f32[1024,3]{1,0:T(8,128)S(1)} %copy.59, f32[1024]{0:T(1024)S(1)} %bitcast.169, f32[1024]{0:T(1024)S(1)} %bitcast.170, f32[1024]{0:T(1024)S(1)} %bitcast.168, f32[1024]{0:T(1024)S(1)} %bitcast.167), kind=kLoop, calls=%fused_computation.63 | loop fusion | flops 5505024 | bytes 3174400 | tf_op jit(solution)/shard_map/jit(silu)/mul | solution.py:50
  45.2 2.6 %reshape_reshape.3 = f32[16,64,3,128]{3,2,1,0:T(4,128)S(1)} reshape(f32[1024,384]{1,0:T(8,128)} %divide_multiply_fusion) | data formatting | bytes 3145728 | tf_op jit(solution)/shard_map/reshape;reshape | solution.py:105
  48.1 14.7 %all-gather.5.cloned.1.call-done = bf16[4,640,512]{2,1,0:T(8,128)(2,1)} async-done(((bf16[1,640,512]{2,1,0:T(8,128)(2,1)}), bf16[4,640,512]{2,1,0:T(8,128)(2,1)}) %all-gather.5.cloned.1.call-update) | async-done | bytes 2621456 | tf_op jit(solution)/shard_map/all_gather | solution.py:170
  62.8 4.4 %copy.71 = bf16[4,640,512]{1,2,0:T(8,128)(2,1)} copy(bf16[4,640,512]{2,1,0:T(8,128)(2,1)} %all-gather.5.cloned.1.call-done) | data formatting | bytes 5242880 | tf_op jit(solution)/shard_map/all_gather | solution.py:170
  67.2 7.0 %fusion.18 = f32[640,1280]{1,0:T(8,128)S(1)} fusion(bf16[640,2048]{0,1:T(8,128)(2,1)} %bitcast.154, bf16[1,2048,1280]{2,1,0:T(8,128)(2,1)} %param.35), kind=kOutput, calls=%fused_computation.35 | convolution fusion | flops 3355443200 | bytes 11141120 | tf_op jit(solution)/shard_map/dot_general | solution.py:173
  74.3 6.5 %fusion.26 = bf16[640,1280]{1,0:T(8,128)(2,1)S(1)} fusion(bf16[640,2048]{0,1:T(8,128)(2,1)S(1)} %bitcast.155, bf16[1,2048,1280]{2,1,0:T(8,128)(2,1)} %param.36, f32[640,1280]{1,0:T(8,128)S(1)} %fusion.18), kind=kOutput, calls=%fused_computation.39 | convolution fusion | flops 3360358400 | bytes 12779520 | tf_op jit(solution)/shard_map/dot_general | solution.py:174
  80.9 4.8 %fusion.29 = bf16[2048,640]{0,1:T(8,128)(2,1)} fusion(bf16[640,1280]{1,0:T(8,128)(2,1)S(1)} %fusion.26, bf16[1,1280,2048]{2,1,0:T(8,128)(2,1)S(1)} %bitcast.174), kind=kOutput, calls=%fused_computation.40 | convolution fusion | flops 3356753920 | bytes 9502720 | tf_op jit(solution)/shard_map/dot_general | solution.py:178
  86.0 36.9 %while.26 = (s32[]{:T(128)}, f32[16,64,128]{2,1,0:T(8,128)S(1)}, f32[3,16,64,128]{3,2,1,0:T(8,128)}, f32[3,16,128]{2,0,1:T(4,128)}, f32[3,16,64,128]{3,0,2,1:T(4...) while((s32[]{:T(128)}, f32[16,64,128]{2,1,0:T(8,128)S(1)}, ...), condition=%wide.region_2.3_spmd.clone, body=%wide.region_0.2_spmd.clone.sunk | while | flops 1008879616 | bytes 9881236 | solution.py:117
  86.0 0.9 constant_dynamic-slice_fusion.14
  87.4 0.6 fusion.101
  88.1 1.6 fusion.102
  89.9 2.7 %fusion.103 = f32[16,128,128]{2,1,0:T(8,128)S(1)} fusion(f32[16,128]{1,0:T(8,128)} %bitcast.164, f32[16,128]{1,0:T(8,128)S(1)} %reduce_window_sum.51, f32[128,128]{1,0:T(8,128)S(1)} %bitcast.153, f32[128,128]{1,0:T(8,128)S(1)} %bitcast.150, pred[128,128]{1,0:T(8,128)(4,1)S(1)} %iota_compare_fusion.4), kind=kOutput, calls=%fused_computation.6.clone.1 | convolution fusion | flops 403701760 | bytes 1212416 | tf_op jit(solution)/shard_map/while/body/eval_jaxpr/hnt,hns->hts/dot_general | solution.py:59
  92.6 0.6 constant_dynamic-slice_fusion.13
  93.2 3.0 %fusion.104 = f32[3,16,64,128]{3,2,1,0:T(8,128)} fusion(f32[3,16,64,128]{3,2,1,0:T(8,128)} %get-tuple-element.306, s32[]{:T(128)} %get-tuple-element.304, f32[16,64,128]{2,1,0:T(8,128)S(1)} %fusion.102, f32[16,64,128]{2,1,0:T(8,128)S(1)} %bitcast.146, f32[16,128,128]{2,1,0:T(8,128)S(1)} %fusion.103), kind=kOutput, calls=%fused_computation.11.clone.1 | convolution fusion | flops 201457664 | bytes 2621952 | tf_op jit(solution)/shard_map/while/body/eval_jaxpr/hts,hps->hpt/dot_general | solution.py:63
  96.1 2.1 %convolution_add_fusion.3 = f32[16,64,128]{2,1,0:T(8,128)S(1)} fusion(f32[128,128]{1,0:T(8,128)S(1)} %bitcast.151, f32[16,64,128]{2,1,0:T(8,128)S(1)} %bitcast.147, f32[16,64,128]{2,1,0:T(8,128)S(1)} %get-tuple-element.305, f32[16,128]{1,0:T(8,128)S(1)} %get-tuple-element.290, f32[16]{0:T(128)S(1)} %exp.116, pred[]{:T(512)S(6)} %compare.10), kind=kOutput, calls=%fused_computation.12.clone.1 | convolution fusion | flops 201850880 | bytes 1646657 | tf_op jit(solution)/shard_map/while/body/eval_jaxpr/hps,hns->hpn/dot_general | solution.py:69
  98.3 0.9 constant_dynamic-slice_fusion.14
  99.7 0.6 fusion.101
  100.4 1.6 fusion.102
  102.2 2.7 %fusion.103 = f32[16,128,128]{2,1,0:T(8,128)S(1)} fusion(f32[16,128]{1,0:T(8,128)} %bitcast.164, f32[16,128]{1,0:T(8,128)S(1)} %reduce_window_sum.51, f32[128,128]{1,0:T(8,128)S(1)} %bitcast.153, f32[128,128]{1,0:T(8,128)S(1)} %bitcast.150, pred[128,128]{1,0:T(8,128)(4,1)S(1)} %iota_compare_fusion.4), kind=kOutput, calls=%fused_computation.6.clone.1 | convolution fusion | flops 403701760 | bytes 1212416 | tf_op jit(solution)/shard_map/while/body/eval_jaxpr/hnt,hns->hts/dot_general | solution.py:59
  104.9 0.6 constant_dynamic-slice_fusion.13
  105.5 3.0 %fusion.104 = f32[3,16,64,128]{3,2,1,0:T(8,128)} fusion(f32[3,16,64,128]{3,2,1,0:T(8,128)} %get-tuple-element.306, s32[]{:T(128)} %get-tuple-element.304, f32[16,64,128]{2,1,0:T(8,128)S(1)} %fusion.102, f32[16,64,128]{2,1,0:T(8,128)S(1)} %bitcast.146, f32[16,128,128]{2,1,0:T(8,128)S(1)} %fusion.103), kind=kOutput, calls=%fused_computation.11.clone.1 | convolution fusion | flops 201457664 | bytes 2621952 | tf_op jit(solution)/shard_map/while/body/eval_jaxpr/hts,hps->hpt/dot_general | solution.py:63
  108.4 2.1 %convolution_add_fusion.3 = f32[16,64,128]{2,1,0:T(8,128)S(1)} fusion(f32[128,128]{1,0:T(8,128)S(1)} %bitcast.151, f32[16,64,128]{2,1,0:T(8,128)S(1)} %bitcast.147, f32[16,64,128]{2,1,0:T(8,128)S(1)} %get-tuple-element.305, f32[16,128]{1,0:T(8,128)S(1)} %get-tuple-element.290, f32[16]{0:T(128)S(1)} %exp.116, pred[]{:T(512)S(6)} %compare.10), kind=kOutput, calls=%fused_computation.12.clone.1 | convolution fusion | flops 201850880 | bytes 1646657 | tf_op jit(solution)/shard_map/while/body/eval_jaxpr/hps,hns->hpn/dot_general | solution.py:69
  110.6 0.9 constant_dynamic-slice_fusion.14
  111.9 0.6 fusion.101
  112.7 1.6 fusion.102
  114.5 2.7 %fusion.103 = f32[16,128,128]{2,1,0:T(8,128)S(1)} fusion(f32[16,128]{1,0:T(8,128)} %bitcast.164, f32[16,128]{1,0:T(8,128)S(1)} %reduce_window_sum.51, f32[128,128]{1,0:T(8,128)S(1)} %bitcast.153, f32[128,128]{1,0:T(8,128)S(1)} %bitcast.150, pred[128,128]{1,0:T(8,128)(4,1)S(1)} %iota_compare_fusion.4), kind=kOutput, calls=%fused_computation.6.clone.1 | convolution fusion | flops 403701760 | bytes 1212416 | tf_op jit(solution)/shard_map/while/body/eval_jaxpr/hnt,hns->hts/dot_general | solution.py:59
  117.2 0.6 constant_dynamic-slice_fusion.13
  117.7 3.0 %fusion.104 = f32[3,16,64,128]{3,2,1,0:T(8,128)} fusion(f32[3,16,64,128]{3,2,1,0:T(8,128)} %get-tuple-element.306, s32[]{:T(128)} %get-tuple-element.304, f32[16,64,128]{2,1,0:T(8,128)S(1)} %fusion.102, f32[16,64,128]{2,1,0:T(8,128)S(1)} %bitcast.146, f32[16,128,128]{2,1,0:T(8,128)S(1)} %fusion.103), kind=kOutput, calls=%fused_computation.11.clone.1 | convolution fusion | flops 201457664 | bytes 2621952 | tf_op jit(solution)/shard_map/while/body/eval_jaxpr/hts,hps->hpt/dot_general | solution.py:63
  120.7 2.1 %convolution_add_fusion.3 = f32[16,64,128]{2,1,0:T(8,128)S(1)} fusion(f32[128,128]{1,0:T(8,128)S(1)} %bitcast.151, f32[16,64,128]{2,1,0:T(8,128)S(1)} %bitcast.147, f32[16,64,128]{2,1,0:T(8,128)S(1)} %get-tuple-element.305, f32[16,128]{1,0:T(8,128)S(1)} %get-tuple-element.290, f32[16]{0:T(128)S(1)} %exp.116, pred[]{:T(512)S(6)} %compare.10), kind=kOutput, calls=%fused_computation.12.clone.1 | convolution fusion | flops 201850880 | bytes 1646657 | tf_op jit(solution)/shard_map/while/body/eval_jaxpr/hps,hns->hpn/dot_general | solution.py:69
  122.9 0.7 convert_element_type.96
  123.6 1.3 dynamic-slice
  125.6 0.7 exponential_convert_fusion
  126.5 13.6 %all-reduce.1 = bf16[128]{0:T(256)(128)(2,1)S(1)} all-reduce(bf16[128]{0:T(256)(128)(2,1)S(1)} %dynamic-update-slice), channel_id=2, replica_groups=mesh['ep'=8,'tp'=4] {'ep'}, use_global_device_ids=true, to_apply=%add.1 | all-reduce | flops 128 | bytes 512
  140.2 0.7 copy_bitcast_fusion.1
  141.0 0.9 reduce-window.14
  142.0 0.8 mul.348
  142.8 0.7 rev.3
  143.5 0.7 add_divide_fusion
  144.3 0.7 pad_clamp_fusion
  145.1 7.9 %all-to-all-start.1 = ((bf16[512,8,80]{0,2,1:T(8,128)(2,1)}), bf16[512,8,80]{0,2,1:T(8,128)(2,1)S(1)}, u32[]{:S(2)}, u32[]{:S(2)}) async-start(bf16[512,8,80]{0,2,1:T(8,128)(2,1)} %bitcast.166), calls=%async_computation.2 | async-start | bytes 1310720 | tf_op jit(solution)/shard_map/all_to_all | solution.py:186
  153.1 30.2 %all-gather.7.cloned.1.call-done = bf16[128,64,128]{2,1,0:T(8,128)(2,1)} async-done(((bf16[16,64,128]{2,1,0:T(8,128)(2,1)}), bf16[128,64,128]{2,1,0:T(8,128)(2,1)}) %all-gather.7.cloned.1.call-update) | async-done | bytes 2097168 | tf_op jit(solution)/shard_map/all_gather | solution.py:26
  183.3 8.2 %while.25 = (s32[]{:T(128)}, f32[16,64,128]{2,1,0:T(8,128)S(1)}, s32[]{:T(128)}, bf16[8,16]{1,0:T(8,128)(2,1)S(1)}, bf16[8,16,64,128]{3,2,1,0:T(8,128)(2,1)}, /*index=5*/s32[]{:T(128)}, s32[]{:T(128)}, s32[]{:T(128)}) while((s32[]{:T(128)}, f32[16,64,128]{2,1,0:T(8,128)S(1)}, s32[]{:T(128)}, bf16[8,16]{1,0:T(8,128)(2,1)S(1)}, ...), condition=%wide.region_5.6_spmd, body=%wide.region_4.5_spmd.sunk | while | flops 393237 | bytes 1311007 | solution.py:40
  183.4 1.2 convert_add_fusion.2
  184.6 1.1 convert_add_fusion.2
  185.8 1.1 convert_add_fusion.2
  187.0 1.1 convert_add_fusion.2
  188.1 1.1 convert_add_fusion.2
  189.3 1.1 convert_add_fusion.2
  190.4 1.1 convert_add_fusion.2
  191.6 3.0 %multiply_reduce_fusion = (f32[16,384]{1,0:T(8,128)S(1)}, f32[16,64,384]{2,1,0:T(8,128)S(1)}) fusion(bf16[16,64,384]{2,1,0:T(8,128)(2,1)} %bitcast.175, f32[16,384]{1,0:T(8,128)S(1)} %copy_bitcast_fusion, f32[16,64,128]{2,1,0:T(8,128)S(1)} %get-tuple-element.91, f32[128,384]{0,1:T(8,128)S(1)} %bitcast.159, f32[3,16,64,128]{3,2,1,0:T(8,128)S(1)} %copy-done.20), kind=kOutput, calls=%fused_computation.62 | convolution fusion | flops 607905792 | bytes 4702208 | tf_op jit(solution)/shard_map/nt,hpn->hpt/dot_general | solution.py:132
  194.6 1.1 multiply_convert_fusion
  195.8 2.0 gather_fusion
  197.9 0.4 reshape.251
  198.3 1.5 multiply_reduce_fusion.2
  (151 shorter events, 6.0 us)
Async XLA Ops:
  8.0 1.3 copy-start.1
  8.0 1.6 copy-start.14
  8.0 54.8 %all-gather.5.cloned.1.call-start = ((), (), s32[]{:S(2)}) async-start(), calls=%async_computation.3 | async-start | bytes 3276800 | tf_op jit(solution)/shard_map/all_gather | solution.py:170
  11.4 25.2 %copy-start.13 = (s32[320]{0:T(512)}, s32[320]{0:T(512)S(1)}, u32[]{:S(2)}) copy-start(s32[320]{0:T(512)S(1)} %get-tuple-element.194) | copy-start | bytes 3844
  12.2 24.5 %copy-start.9 = (bf16[256,384]{1,0:T(8,128)(2,1)S(1)}, bf16[256,384]{1,0:T(8,128)(2,1)}, u32[]{:S(2)}) copy-start(bf16[256,384]{1,0:T(8,128)(2,1)} %param.26) | copy-start | bytes 589828
  12.2 24.5 %copy-start.10 = (bf16[256,384]{1,0:T(8,128)(2,1)S(1)}, bf16[256,384]{1,0:T(8,128)(2,1)}, u32[]{:S(2)}) copy-start(bf16[256,384]{1,0:T(8,128)(2,1)} %param.25) | copy-start | bytes 589828
  12.3 24.7 %copy-start.2 = (bf16[1024,384]{1,0:T(8,128)(2,1)S(1)}, bf16[1024,384]{1,0:T(8,128)(2,1)}, u32[]{:S(2)}) copy-start(bf16[1024,384]{1,0:T(8,128)(2,1)} %param.21) | copy-start | bytes 2359300
  15.7 23.1 %copy-start.17 = (f32[256,4]{0,1:T(4,128)S(1)}, f32[256,4]{0,1:T(4,128)}, u32[]{:S(2)}) copy-start(f32[256,4]{0,1:T(4,128)} %param.29) | copy-start | bytes 12292
  15.7 23.1 %copy-start.18 = (f32[256,4]{0,1:T(4,128)S(1)}, f32[256,4]{0,1:T(4,128)}, u32[]{:S(2)}) copy-start(f32[256,4]{0,1:T(4,128)} %param.28) | copy-start | bytes 12292
  15.7 23.1 %copy-start.12 = (f32[1024,4]{0,1:T(4,128)S(1)}, f32[1024,4]{0,1:T(4,128)}, u32[]{:S(2)}) copy-start(f32[1024,4]{0,1:T(4,128)} %param.27) | copy-start | bytes 49156
  15.7 23.1 %copy-start.11 = (f32[16,384]{1,0:T(8,128)S(1)}, f32[16,384]{1,0:T(8,128)}, u32[]{:S(2)}) copy-start(f32[16,384]{1,0:T(8,128)} %param.23) | copy-start | bytes 73732
  15.7 23.1 %copy-start.19 = (f32[16]{0:T(128)S(1)}, f32[16]{0:T(128)}, u32[]{:S(2)}) copy-start(f32[16]{0:T(128)} %param.24) | copy-start | bytes 196
  36.6 108.6 %reduce-scatter.2.cloned.1.call-start = ((), (), s32[]{:S(2)}) async-start(), calls=%async_computation.4 | async-start | bytes 3276800 | tf_op jit(solution)/shard_map/reduce_scatter | solution.py:177
  37.3 4.4 %collective-permute-start = (bf16[1280,3]{0,1:T(4,128)(2,1)S(1)}, bf16[1280,3]{0,1:T(4,128)(2,1)S(1)}, u32[]{:S(2)}, u32[]{:S(2)}) collective-permute-start(bf16[1280,3]{0,1:T(4,128)(2,1)S(1)} %pad_maximum_fusion.3), channel_id=1, source_target_pairs={{0,4},{4,8},{8,12},{12,16},{16,20},{20,24},{24,28},{1,5},{5,9},{9,... | collective-permute-start | bytes 23048 | tf_op jit(solution)/shard_map/ppermute | solution.py:20
  39.6 2.3 %copy-start.6 = (f32[16,384]{1,0:T(8,128)}, f32[16,384]{1,0:T(8,128)S(1)}, u32[]{:S(2)}) copy-start(f32[16,384]{1,0:T(8,128)S(1)} %get-tuple-element.170) | copy-start | bytes 73732
  45.2 2.8 %copy-start.15 = (f32[128]{0:T(128)S(1)}, f32[128]{0:T(128)}, u32[]{:S(2)}) copy-start(f32[128]{0:T(128)} %get-tuple-element.186) | copy-start | bytes 1540
  45.2 2.8 %copy-start.16 = (f32[128]{0:T(128)S(1)}, f32[128]{0:T(128)}, u32[]{:S(2)}) copy-start(f32[128]{0:T(128)} %get-tuple-element.187) | copy-start | bytes 1540
  67.2 7.1 %copy-start = (bf16[4,640,512]{1,2,0:T(8,128)(2,1)S(1)}, bf16[4,640,512]{1,2,0:T(8,128)(2,1)}, u32[]{:S(2)}) copy-start(bf16[4,640,512]{1,2,0:T(8,128)(2,1)} %copy.71) | copy-start | bytes 7864324
  67.2 13.6 %slice-start = ((s8[5242880]{0:T(1024)(128)(4,1)}), s8[4194304]{0:T(1024)(128)(4,1)S(1)}, s32[]{:S(2)}) async-start(s8[5242880]{0:T(1024)(128)(4,1)} %bitcast.173), calls=%async_computation.6 | async-start | bytes 8388608
  74.3 6.6 %slice-start.1 = ((s8[5242880]{0:T(1024)(128)(4,1)}), s8[1048576]{0:T(1024)(128)(4,1)S(1)}, s32[]{:S(2)}) async-start(s8[5242880]{0:T(1024)(128)(4,1)} %bitcast.173), calls=%async_computation.7 | async-start | bytes 2097152
  85.7 97.6 %all-gather.7.cloned.1.call-start = ((), (), s32[]{:S(2)}) async-start(), calls=%async_computation.5 | async-start | bytes 2359296 | tf_op jit(solution)/shard_map/all_gather | solution.py:26
  86.0 2.1 %copy-start.3 = (f32[3,128,128]{1,2,0:T(8,128)}, f32[3,128,128]{1,2,0:T(8,128)S(1)}, u32[]{:S(2)}) copy-start(f32[3,128,128]{1,2,0:T(8,128)S(1)} %get-tuple-element.321) | copy-start | bytes 589828 | tf_op jit(solution)/shard_map/while
  86.9 1.1 copy-start.5
  87.4 0.6 copy-start.7
  93.2 3.0 %copy-start.8 = (f32[16]{0:T(128)S(1)}, f32[16]{0:T(128)}, u32[]{:S(2)}) copy-start(f32[16]{0:T(128)} %copy-done.7) | copy-start | bytes 196 | tf_op jit(solution)/shard_map/while
  96.1 2.1 %copy-start.4 = (f32[3,128,128]{1,2,0:T(8,128)S(1)}, f32[3,128,128]{1,2,0:T(8,128)}, u32[]{:S(2)}) copy-start(f32[3,128,128]{1,2,0:T(8,128)} %copy-done.3) | copy-start | bytes 589828 | tf_op jit(solution)/shard_map/while
  98.3 2.1 %copy-start.3 = (f32[3,128,128]{1,2,0:T(8,128)}, f32[3,128,128]{1,2,0:T(8,128)S(1)}, u32[]{:S(2)}) copy-start(f32[3,128,128]{1,2,0:T(8,128)S(1)} %get-tuple-element.321) | copy-start | bytes 589828 | tf_op jit(solution)/shard_map/while
  99.2 1.1 copy-start.5
  99.6 0.6 copy-start.7
  105.4 3.0 %copy-start.8 = (f32[16]{0:T(128)S(1)}, f32[16]{0:T(128)}, u32[]{:S(2)}) copy-start(f32[16]{0:T(128)} %copy-done.7) | copy-start | bytes 196 | tf_op jit(solution)/shard_map/while
  108.4 2.1 %copy-start.4 = (f32[3,128,128]{1,2,0:T(8,128)S(1)}, f32[3,128,128]{1,2,0:T(8,128)}, u32[]{:S(2)}) copy-start(f32[3,128,128]{1,2,0:T(8,128)} %copy-done.3) | copy-start | bytes 589828 | tf_op jit(solution)/shard_map/while
  110.6 2.1 %copy-start.3 = (f32[3,128,128]{1,2,0:T(8,128)}, f32[3,128,128]{1,2,0:T(8,128)S(1)}, u32[]{:S(2)}) copy-start(f32[3,128,128]{1,2,0:T(8,128)S(1)} %get-tuple-element.321) | copy-start | bytes 589828 | tf_op jit(solution)/shard_map/while
  111.5 1.1 copy-start.5
  111.9 0.6 copy-start.7
  117.7 3.0 %copy-start.8 = (f32[16]{0:T(128)S(1)}, f32[16]{0:T(128)}, u32[]{:S(2)}) copy-start(f32[16]{0:T(128)} %copy-done.7) | copy-start | bytes 196 | tf_op jit(solution)/shard_map/while
  120.7 2.1 %copy-start.4 = (f32[3,128,128]{1,2,0:T(8,128)S(1)}, f32[3,128,128]{1,2,0:T(8,128)}, u32[]{:S(2)}) copy-start(f32[3,128,128]{1,2,0:T(8,128)} %copy-done.3) | copy-start | bytes 589828 | tf_op jit(solution)/shard_map/while
  145.1 50.6 %all-to-all-start.1 = ((bf16[512,8,80]{0,2,1:T(8,128)(2,1)}), bf16[512,8,80]{0,2,1:T(8,128)(2,1)S(1)}, u32[]{:S(2)}, u32[]{:S(2)}) async-start(bf16[512,8,80]{0,2,1:T(8,128)(2,1)} %bitcast.166), calls=%async_computation.2 | async-start | bytes 1310720 | tf_op jit(solution)/shard_map/all_to_all | solution.py:186
  183.3 8.3 %copy-start.20 = (f32[3,16,64,128]{3,2,1,0:T(8,128)S(1)}, f32[3,16,64,128]{3,2,1,0:T(8,128)}, u32[]{:S(2)}) copy-start(f32[3,16,64,128]{3,2,1,0:T(8,128)} %get-tuple-element.89) | copy-start | bytes 4718596
Sparse Core Ops, SparseCore 0:
  36.7 26.0 all-gather.4
  85.8 33.8 reduce-scatter.1
Sparse Core Ops, SparseCore 1:
  123.7 59.5 all-gather.6
